TPU v7x, 32 devices: a whole 2x2x4 slice. The times are simulated.
32 devices in a mesh: grp: 2 (over y), kv: 4 (over z), tp: 4 (over x, core).
Axes of the slice: x: 2, y: 2, z: 4, core: 2. Of those that a mesh axis runs over, the one named last changes fastest.
Arguments:
- piece_rows: bfloat16 [512, 2048], P(('grp', 'kv')), parts along dimension 0, may hold values from -6 to 6
- dec_rows: bfloat16 [16, 2048], P(('grp', 'kv')), parts along dimension 0, may hold values from -6 to 6
- norm_gain: float32 [2048], replicated, may hold values from 0.1 to 1.9
- w_query: bfloat16 [2048, 1024], P(None, 'tp'), may hold values from -0.25 to 0.25
- w_key: bfloat16 [2048, 256], P(None, 'tp'), may hold values from -0.125 to 0.125
- w_value: bfloat16 [2048, 256], P(None, 'tp'), may hold values from -0.125 to 0.125
- w_forget: bfloat16 [2048, 16], P(None, 'tp'), may hold values from -0.125 to 0.125
- forget_bias: float32 [16], P('tp'), may hold values from 3 to 12
- piece_decay: float32 [16, 512], P('tp', ('grp', 'kv')), parts along dimension 1, may hold values from -3 to 0
- cache_kv: bfloat16 [6144, 4, 128], P(('grp', 'kv'), 'tp'), parts along dimension 0, may hold values from -150 to 150
- cache_gate: float32 [16, 6144], P('tp', ('grp', 'kv')), parts along dimension 1, may hold values from -156.6 to 0, as said below
- dec_cache: bfloat16 [16, 3072, 4, 128], P(('grp', 'kv'), None, 'tp'), parts along dimension 0, may hold values from -150 to 150
- dec_gate: float32 [16, 16, 3072], P(('grp', 'kv'), 'tp'), parts along dimension 0, may hold values from -156.6 to 0, as said below
- dec_lengths: int32 [16], P(('grp', 'kv')), parts along dimension 0, may hold values from 1 to 3072, as said below
- w_out: bfloat16 [1024, 2048], P(None, 'tp'), may hold values from -0.75 to 0.75
Outputs:
- piece_out: bfloat16 [512, 2048], P(('grp', 'kv'), 'tp'), parts along dimension 0
- dec_out: bfloat16 [16, 2048], P(('grp', 'kv'), 'tp'), parts along dimension 0
There are 2 independent parts, one for each index of `grp`. A program takes and returns all parts, laid end to end along the dimension named above; an argument that names none is the same for every part. Nothing has to cross between parts.
Inputs may be any that keep to these rules, and one draw needn't show every extreme that they name: `cache_gate`: each head's values never fall from one position to the next and are 0 at the last cached position. `dec_gate`: each sequence's and head's values never rise from one position to the next. Sequence b's cache holds its first dec_lengths[b] positions; in each part some sequence holds 3072.
All inputs are finite; a program needn't handle non-finite values.
Results may differ from a plain program's by a relative error of at most 0.006.
The roundings to bfloat16 on the way count: a program that leaves them out, or rounds other values in their place, can miss the bound.
Values may be sent and summed in bfloat16 or wider, within the bound.
A program may use at most 64 MiB of HBM per device.

v0:
```python
import jax
import jax.numpy as jnp
from jax import lax
from jax.sharding import PartitionSpec as P


def carried_in(array, axis, combine, identity):
    length, mine = (lax.axis_size(axis), lax.axis_index(axis))
    everything = lax.all_gather(array, axis)
    start = jnp.broadcast_to(jnp.asarray(identity, array.dtype), array.shape)

    def lap(k, before):
        reached = k < mine
        new = combine(before, everything[k])
        return jnp.where(reached, new, before)

    return lax.fori_loop(0, length, lap, start)


def norm_rows(rows, gain):
    wide = rows.astype(jnp.float32)
    scale = lax.rsqrt(jnp.mean(wide * wide, axis=-1, keepdims=True) + 1e-06)
    return (wide * scale * gain).astype(jnp.bfloat16)


def add_terms(earlier, later):
    return earlier + later


def merge_state(state, part):
    peak, total, numer = state
    new_peak, new_total, new_numer = part
    highest = jnp.maximum(peak, new_peak)
    keep = jnp.exp(peak - highest)
    fresh = jnp.exp(new_peak - highest)
    return (
        highest,
        total * keep + new_total * fresh,
        numer * keep[..., None] + new_numer * fresh[..., None],
    )


def group_partial(query, query_index, group_kv, group_bias, group, past_rows, new_rows):
    head_width = query.shape[-1]
    keys = group_kv[..., :head_width]
    values = group_kv[..., head_width:]
    score = jnp.einsum("bkgd,nkd->bkgn", query, keys, preferred_element_type=jnp.float32)
    score = score * head_width ** (-0.5) + group_bias[None]
    rank = jnp.arange(group_kv.shape[0], dtype=jnp.int32)
    new_index = group * new_rows + rank - past_rows
    visible = (rank < past_rows)[None, :] | (new_index[None, :] <= query_index[:, None])
    score = jnp.where(visible[:, None, None, :], score, -jnp.inf)
    peak = jnp.max(score, axis=-1)
    weight = jnp.exp(score - peak[..., None])
    total = jnp.sum(weight, axis=-1)
    numer = jnp.einsum(
        "bkgn,nkd->bkgd", weight.astype(jnp.bfloat16), values, preferred_element_type=jnp.float32
    )
    return (peak, total, numer)


def decode_attention(query, new_key, new_value, new_gate, cache, gate, lengths):
    seqs, pairs_here, group_size, head_width = query.shape
    span = cache.shape[1]
    keys = cache[..., :head_width]
    values = cache[..., head_width:]
    target_location = jnp.arange(span, dtype=jnp.int32)
    last_gate = jnp.sum(
        jnp.where(target_location[None, None, :] == lengths[:, None, None] - 1, gate, 0.0), axis=-1
    )
    score = jnp.einsum(
        "skgd,slkd->skgl", query, keys, preferred_element_type=jnp.float32
    ) * head_width ** (-0.5)
    score = score - gate.reshape(seqs, pairs_here, group_size, span)
    score = jnp.where(
        (target_location[None, :] < lengths[:, None])[:, None, None, :], score, -jnp.inf
    )
    own = jnp.einsum(
        "skgd,skd->skg", query, new_key, preferred_element_type=jnp.float32
    ) * head_width ** (-0.5)
    own = own - (last_gate + new_gate).reshape(seqs, pairs_here, group_size)
    peak = jnp.maximum(jnp.max(score, axis=-1), own)
    weight = jnp.exp(score - peak[..., None])
    own_weight = jnp.exp(own - peak)
    total = jnp.sum(weight, axis=-1) + own_weight
    numer = jnp.einsum(
        "skgl,slkd->skgd", weight.astype(jnp.bfloat16), values, preferred_element_type=jnp.float32
    )
    numer = numer + own_weight.astype(jnp.bfloat16).astype(jnp.float32)[..., None] * new_value[
        :, :, None, :
    ].astype(jnp.float32)
    return numer / total[..., None]


def local(
    piece_rows,
    dec_rows,
    norm_gain,
    w_query,
    w_key,
    w_value,
    w_forget,
    forget_bias,
    piece_decay,
    cache_kv,
    cache_gate,
    dec_cache,
    dec_gate,
    dec_lengths,
    w_out,
):
    piece_count = piece_rows.shape[0]
    dec_count = dec_rows.shape[0]
    past_rows = cache_kv.shape[0]
    pairs_here = cache_kv.shape[1]
    head_width = cache_kv.shape[2] // 2
    heads_here = w_forget.shape[1]
    group_size = heads_here // pairs_here
    group_rows = past_rows + piece_count
    normed = norm_rows(jnp.concatenate([piece_rows, dec_rows], axis=0), norm_gain)
    query = jnp.dot(normed, w_query, preferred_element_type=jnp.float32).astype(jnp.bfloat16)
    new_key = jnp.dot(normed, w_key, preferred_element_type=jnp.float32).astype(jnp.bfloat16)
    new_value = jnp.dot(normed, w_value, preferred_element_type=jnp.float32).astype(jnp.bfloat16)
    log_gate = jax.nn.log_sigmoid(
        jnp.dot(normed, w_forget, preferred_element_type=jnp.float32) + forget_bias
    )
    piece_gate = log_gate[:piece_count] + piece_decay.T
    running = jnp.cumsum(piece_gate, axis=0)
    before = carried_in(running[-1], "kv", add_terms, jnp.zeros((heads_here,), jnp.float32))
    new_bias = -(running + before[None, :]).T
    piece_kv = jnp.concatenate(
        [
            new_key[:piece_count].reshape(piece_count, pairs_here, head_width),
            new_value[:piece_count].reshape(piece_count, pairs_here, head_width),
        ],
        axis=-1,
    )
    group_kv = jnp.concatenate([cache_kv, piece_kv], axis=0)
    group_bias = jnp.concatenate([cache_gate, new_bias], axis=1)
    my_group = lax.axis_index("kv")
    every_bias = lax.all_gather(group_bias, "kv", axis=1, tiled=True)
    own_query = query[:piece_count].reshape(piece_count, pairs_here, group_size, head_width)
    own_index = my_group * piece_count + jnp.arange(piece_count, dtype=jnp.int32)
    start_state = (
        jnp.full((piece_count, pairs_here, group_size), -jnp.inf, jnp.float32),
        jnp.zeros((piece_count, pairs_here, group_size), jnp.float32),
        jnp.zeros((piece_count, pairs_here, group_size, head_width), jnp.float32),
    )
    state = start_state
    piece = lax.all_gather(group_kv, "kv", axis=0, tiled=True)
    count = piece.shape[0] // group_rows
    blocks = piece.reshape(count, group_rows, pairs_here, 2 * head_width)

    def visit(carry, item):
        block, offset = item
        bias = lax.dynamic_slice_in_dim(every_bias, offset * group_rows, group_rows, 1)
        part = group_partial(
            own_query,
            own_index,
            block,
            bias.reshape(pairs_here, group_size, group_rows),
            offset,
            past_rows,
            piece_count,
        )
        return (merge_state(carry, part), None)

    state, _ = lax.scan(visit, state, (blocks, jnp.arange(count, dtype=jnp.int32)))
    peak, total, numer = state
    piece_attn = numer / total[..., None]
    dec_attn = decode_attention(
        query[piece_count:].reshape(dec_count, pairs_here, group_size, head_width),
        new_key[piece_count:].reshape(dec_count, pairs_here, head_width),
        new_value[piece_count:].reshape(dec_count, pairs_here, head_width),
        log_gate[piece_count:],
        dec_cache,
        dec_gate,
        dec_lengths,
    )
    attn_rows = jnp.concatenate(
        [
            piece_attn.reshape(piece_count, heads_here * head_width),
            dec_attn.reshape(dec_count, heads_here * head_width),
        ],
        axis=0,
    ).astype(jnp.bfloat16)
    every_head = lax.all_gather(attn_rows, "tp", axis=1, tiled=True)
    mixed = jnp.dot(every_head, w_out, preferred_element_type=jnp.float32).astype(jnp.bfloat16)
    return (mixed[:piece_count], mixed[piece_count:])


def solution(mesh):
    return jax.shard_map(
        local,
        mesh=mesh,
        in_specs=(
            P(("grp", "kv"), None),
            P(("grp", "kv"), None),
            P(),
            P(None, "tp"),
            P(None, "tp"),
            P(None, "tp"),
            P(None, "tp"),
            P("tp"),
            P("tp", ("grp", "kv")),
            P(("grp", "kv"), "tp", None),
            P("tp", ("grp", "kv")),
            P(("grp", "kv"), None, "tp", None),
            P(("grp", "kv"), "tp", None),
            P(("grp", "kv")),
            P(None, "tp"),
        ),
        out_specs=(P(("grp", "kv"), "tp"), P(("grp", "kv"), "tp")),
        check_vma=False,
    )
```

profile of v0, /device:TPU:0, one launch (start us, length us, event | category | flops | bytes accessed | tf_op | source)
XLA Modules:
  0.0 78.9 jit_solution(7893295334877088448)
XLA Ops:
  0.7 0.8 broadcast_add_fusion
  1.5 1.1 %fusion.35 = f32[66]{0:T(128)S(1)} fusion(bf16[2,2048]{1,0:T(2,128)(2,1)} %param.20, bf16[64,2048]{1,0:T(8,128)(2,1)} %param.19), kind=kLoop, calls=%fused_computation.54 | loop fusion | flops 810942 | bytes 270600 | tf_op jit(solution)/shard_map/reduce_sum | solution.py:22
  2.6 1.3 %fusion.42 = f32[66,4]{0,1:T(4,128)S(1)} fusion(bf16[2048,4]{0,1:T(4,128)(2,1)} %param.25, f32[4]{0:T(128)} %param.26, f32[2048]{0:T(1024)} %param.21, f32[66]{0:T(128)S(1)} %add_rsqrt_fusion, bf16[2,2048]{1,0:T(2,128)(2,1)} %param.20, bf16[64,2048]{1,0:T(8,128)(2,1)} %param.19), kind=kOutput, calls=%fused_computation.73 | convolution fusion | flops 2029896 | bytes 296248 | tf_op jit(solution)/shard_map/dot_general | solution.py:125
  3.9 0.7 bitcast_add_fusion
  4.7 1.0 %select_reduce_fusion = f32[2,4]{1,0:T(2,128)S(1)} fusion(f32[2,4,3072]{2,1,0:T(4,128)} %param.31, pred[2,3072]{1,0:T(4,128)(4,1)S(1)} %iota_compare_fusion.1), kind=kLoop, calls=%fused_computation.61 | loop fusion | flops 49144 | bytes 104480 | tf_op jit(solution)/shard_map/reduce_sum | solution.py:68
  5.8 0.7 iota_compare_fusion.2
  6.6 1.4 %convolution_convert_fusion.2 = bf16[66,64]{1,0:T(8,128)(2,1)S(1)} fusion(bf16[2048,64]{0,1:T(8,128)(2,1)} %param.24, f32[2048]{0:T(1024)} %param.21, f32[66]{0:T(128)S(1)} %add_rsqrt_fusion, bf16[2,2048]{1,0:T(2,128)(2,1)} %param.20, bf16[64,2048]{1,0:T(8,128)(2,1)} %param.19), kind=kOutput, calls=%fused_computation.45 | convolution fusion | flops 18251904 | bytes 549384 | tf_op jit(solution)/shard_map/dot_general | solution.py:123
  8.6 12.8 %all-gather = f32[4,1,4]{2,1,0:T(1,128)S(1)} all-gather(f32[1,1,4]{2,1,0:T(1,128)S(1)} %slice_bitcast_fusion.7), channel_id=1, replica_groups=mesh['grp'=2,'kv'=4,'tp'=4] {'kv'}, dimensions={0}, use_global_device_ids=true | all-gather | bytes 80 | tf_op jit(solution)/shard_map/all_gather | solution.py:9
  21.6 1.6 %convolution_convert_fusion.1 = bf16[66,256]{1,0:T(8,128)(2,1)S(1)} fusion(bf16[2048,256]{1,0:T(8,128)(2,1)} %param.22, f32[2048]{0:T(1024)S(1)} %copy-done.8, f32[66]{0:T(128)S(1)} %add_rsqrt_fusion, bf16[2,2048]{1,0:T(2,128)(2,1)S(1)} %copy-done.6, bf16[64,2048]{1,0:T(8,128)(2,1)S(1)} %copy-done.3), kind=kOutput, calls=%fused_computation.44 | convolution fusion | flops 70169088 | bytes 1361160 | tf_op jit(solution)/shard_map/dot_general | solution.py:121
  23.6 13.2 %all-gather.1 = f32[4,832,4]{1,2,0:T(4,128)S(1)} all-gather(f32[1,832,4]{1,2,0:T(4,128)S(1)} %maximum_bitcast_fusion), channel_id=1, replica_groups=mesh['grp'=2,'kv'=4,'tp'=4] {'kv'}, dimensions={0}, use_global_device_ids=true | all-gather | bytes 66560 | tf_op jit(solution)/shard_map/all_gather | solution.py:141
  36.9 0.6 fusion.53
  38.3 0.6 fusion.31
  39.2 17.8 %all_gather.12 = bf16[3328,1,128]{2,0,1:T(8,128)(2,1)S(1)} all-gather(bf16[832,1,128]{2,0,1:T(8,128)(2,1)S(1)} %maximum_maximum_fusion), channel_id=1, replica_groups=mesh['grp'=2,'kv'=4,'tp'=4] {'kv'}, dimensions={0}, use_global_device_ids=true | all-gather | bytes 1064960 | tf_op jit(solution)/shard_map/all_gather | solution.py:150
  57.0 14.4 %while.32 = (s32[]{:T(128)}, f32[64,1,4]{0,2,1:T(4,128)S(1)}, f32[64,1,4]{0,2,1:T(4,128)S(1)}, f32[64,1,4,64]{0,3,2,1:T(8,128)S(1)}, s32[4]{0:T(128)S(1)}, /*ind...) while((s32[]{:T(128)}, f32[64,1,4]{0,2,1:T(4,128)S(1)}, ...), condition=%wide.region_7.8_spmd.clone, body=%wide.region_4.7_spmd.clone.sunk | while | flops 56406536 | bytes 4148079 | solution.py:168
  57.0 0.6 dynamic_slice.41
  59.3 0.4 fusion.69
  59.7 0.3 fusion.71
  60.0 0.5 fusion.73
  60.6 0.6 dynamic_slice.41
  62.9 0.4 fusion.69
  63.3 0.3 fusion.71
  63.6 0.5 fusion.73
  64.2 0.6 dynamic_slice.41
  66.5 0.4 fusion.69
  67.3 0.5 fusion.73
  67.8 0.6 dynamic_slice.41
  70.1 0.4 fusion.69
  70.9 0.5 fusion.73
  71.5 5.8 %all_gather.15 = bf16[66,1024]{0,1:T(8,128)(2,1)S(1)} all-gather(bf16[66,256]{0,1:T(8,128)(2,1)S(1)} %pad_maximum_fusion.1), channel_id=1, replica_groups=mesh['grp'=2,'kv'=4,'tp'=4] {'tp'}, dimensions={1}, use_global_device_ids=true | all-gather | bytes 168960 | tf_op jit(solution)/shard_map/all_gather | solution.py:187
  77.3 0.3 convolution_convert_fusion
  77.7 0.6 slice.76
  78.3 0.6 slice.75
  (104 shorter events, 5.0 us)
Async XLA Ops:
  0.6 76.7 %copy-start = (bf16[1024,512]{1,0:T(8,128)(2,1)S(1)}, bf16[1024,512]{1,0:T(8,128)(2,1)}, u32[]{:S(2)}) copy-start(bf16[1024,512]{1,0:T(8,128)(2,1)} %param.33) | copy-start | bytes 3145732
  0.6 7.3 %copy-start.6 = (bf16[2,2048]{1,0:T(2,128)(2,1)S(1)}, bf16[2,2048]{1,0:T(2,128)(2,1)}, u32[]{:S(2)}) copy-start(bf16[2,2048]{1,0:T(2,128)(2,1)} %param.20) | copy-start | bytes 24580
  0.7 7.3 %copy-start.3 = (bf16[64,2048]{1,0:T(8,128)(2,1)S(1)}, bf16[64,2048]{1,0:T(8,128)(2,1)}, u32[]{:S(2)}) copy-start(bf16[64,2048]{1,0:T(8,128)(2,1)} %param.19) | copy-start | bytes 786436
  0.7 7.3 %copy-start.8 = (f32[2048]{0:T(1024)S(1)}, f32[2048]{0:T(1024)}, u32[]{:S(2)}) copy-start(f32[2048]{0:T(1024)} %param.21) | copy-start | bytes 24580
  0.7 7.3 %copy-start.7 = (bf16[2048,64]{0,1:T(8,128)(2,1)S(1)}, bf16[2048,64]{0,1:T(8,128)(2,1)}, u32[]{:S(2)}) copy-start(bf16[2048,64]{0,1:T(8,128)(2,1)} %param.23) | copy-start | bytes 786436
  2.6 18.9 %copy-start.5 = (f32[4,768]{1,0:T(4,128)S(1)}, f32[4,768]{1,0:T(4,128)}, u32[]{:S(2)}) copy-start(f32[4,768]{1,0:T(4,128)} %param.29) | copy-start | bytes 36868
  8.3 28.6 %copy-start.1 = (bf16[2,3072,1,128]{3,1,2,0:T(8,128)(2,1)S(1)}, bf16[2,3072,1,128]{3,1,2,0:T(8,128)(2,1)}, u32[]{:S(2)}) copy-start(bf16[2,3072,1,128]{3,1,2,0:T(8,128)(2,1)} %param.30) | copy-start | bytes 4718596
  8.3 28.6 %copy-start.2 = (f32[2,4,3072]{2,1,0:T(4,128)S(1)}, f32[2,4,3072]{2,1,0:T(4,128)}, u32[]{:S(2)}) copy-start(f32[2,4,3072]{2,1,0:T(4,128)} %param.31) | copy-start | bytes 294916
  36.9 2.2 %copy-start.4 = (bf16[768,1,128]{2,0,1:T(8,128)(2,1)S(1)}, bf16[768,1,128]{2,0,1:T(8,128)(2,1)}, u32[]{:S(2)}) copy-start(bf16[768,1,128]{2,0,1:T(8,128)(2,1)} %param.28) | copy-start | bytes 589828
where the time goes:
time: 79.3 us; the launch traced here: 78.9 us
  blocking collectives  49.5 us (62%)
  matrix products  9.82 us (12%)
  other arithmetic  6.95 us (9%)
  local copies, waits for them, and re-layouts  6.05 us (8%)
  loops' own time  5.61 us (7%)
  between operations  0.95 us (1%)
    all_gather x1, blocking collectives, local(): piece = lax.all_gather(group_kv, 'kv', axis=0, tiled=True)  17.8 us
    all_gather x1, blocking collectives, local(): every_bias = lax.all_gather(group_bias, 'kv', axis=1, tiled=True)  13.2 us
    all_gather x1, blocking collectives, carried_in(): everything = lax.all_gather(array, axis)  12.8 us
    all_gather x1, blocking collectives, local(): every_head = lax.all_gather(attn_rows, 'tp', axis=1, tiled=True)  5.78 us
    another operation x1, loops' own time, local(): lax.scan(visit, state, (blocks, jnp.arange(count, dtype=jnp.int32)))  5.54 us
    dynamic_slice x12, local copies, waits for them, and re-layouts, local(): lax.scan(visit, state, (blocks, jnp.arange(count, dtype=jnp.int32)))  3.1 us
    dot_general x4, matrix products, group_partial(): jnp.einsum('bkgn,nkd->bkgd', weight.astype(jnp.bfloat16), values, preferr...  2.11 us

commit v1 on v0

--- a/solution.py
+++ b/solution.py
@@ -184,7 +184,12 @@
         ],
         axis=0,
     ).astype(jnp.bfloat16)
-    every_head = lax.all_gather(attn_rows, "tp", axis=1, tiled=True)
+    ring = [attn_rows]
+    for hop in range(3):
+        ring.append(lax.ppermute(ring[-1], "tp", [(dev, (dev + 1) % 4) for dev in range(4)]))
+    every_head = jnp.roll(
+        jnp.concatenate(ring[::-1], axis=1), (lax.axis_index("tp") + 1) * ring[0].shape[1], axis=1
+    )
     mixed = jnp.dot(every_head, w_out, preferred_element_type=jnp.float32).astype(jnp.bfloat16)
     return (mixed[:piece_count], mixed[piece_count:])
 

time: 79.3 us -> 82.1 us (1.035)
  waiting for transfers between devices: 0 us -> 11.1 us
  blocking collectives: 49.5 us -> 43.6 us
  other arithmetic: 6.95 us -> 5.63 us
  matrix products: 9.82 us -> 8.67 us
    ppermute x0 -> x3, waiting for transfers between devices: none -> 11.1 us  [local(): lax.ppermute(ring[-1], 'tp', [(dev, (dev + 1) % 4) for dev in range(4)])]
    all_gather x1 -> x0, blocking collectives: 5.78 us -> none  [local(): every_head = lax.all_gather(attn_rows, 'tp', axis=1, tiled=True)]
    dot_general x1, matrix products: 1.57 us -> 0.35 us  [local(): jnp.dot(normed, w_query, preferred_element_type=jnp.float32)]
    dot_general x1, matrix products: 0.3 us -> 1.36 us  [local(): jnp.dot(normed, w_key, preferred_element_type=jnp.float32)]
    dot_general x1, matrix products: 1.29 us -> 0.29 us  [local(): jnp.dot(normed, w_forget, preferred_element_type=jnp.float32) + forget_bias]
    reduce_sum x1, other arithmetic: 1.02 us -> 0.13 us  [decode_attention(): jnp.sum(jnp.where(target_location[None, None, :] == lengths[:, None, None...]
  transfers between devices with their start and end apart: 0 -> 3, of which waited for: 0 -> 3; matrix products, arithmetic and copies ran while one was open for 0% -> 0% of each run, Pallas kernels for 0% -> 0%
where the time goes in v1:
time: 82.1 us; the launch traced here: 81.8 us
  blocking collectives  43.6 us (53%)
  waiting for transfers between devices  11.1 us (14%)
  matrix products  8.67 us (11%)
  local copies, waits for them, and re-layouts  6.15 us (7%)
  other arithmetic  5.63 us (7%)
  loops' own time  5.61 us (7%)
  between operations  1.05 us (1%)
    all_gather x1, blocking collectives, local(): piece = lax.all_gather(group_kv, 'kv', axis=0, tiled=True)  17.8 us
    all_gather x1, blocking collectives, local(): every_bias = lax.all_gather(group_bias, 'kv', axis=1, tiled=True)  13.2 us
    all_gather x1, blocking collectives, carried_in(): everything = lax.all_gather(array, axis)  12.6 us
    ppermute x3, waiting for transfers between devices, local(): lax.ppermute(ring[-1], 'tp', [(dev, (dev + 1) % 4) for dev in range(4)])  11.1 us
    another operation x1, loops' own time, local(): lax.scan(visit, state, (blocks, jnp.arange(count, dtype=jnp.int32)))  5.54 us
    dynamic_slice x12, local copies, waits for them, and re-layouts, local(): lax.scan(visit, state, (blocks, jnp.arange(count, dtype=jnp.int32)))  3.1 us
    dot_general x4, matrix products, group_partial(): jnp.einsum('bkgn,nkd->bkgd', weight.astype(jnp.bfloat16), values, preferr...  2.12 us
  transfers between devices with their start and end apart: 3, of which 3 were waited for; matrix products, arithmetic and copies ran while one was open for 0% of the time, Pallas kernels for 0%

profile of v1, /device:TPU:0, one launch (start us, length us, event | category | flops | bytes accessed | tf_op | source)
XLA Modules:
  0.0 81.8 jit_solution(10960877339099428022)
XLA Ops:
  0.7 0.8 broadcast_add_fusion
  1.5 0.7 iota_compare_fusion.2
  2.3 1.1 %fusion.35 = f32[66]{0:T(128)S(1)} fusion(bf16[2,2048]{1,0:T(2,128)(2,1)} %param.20, bf16[64,2048]{1,0:T(8,128)(2,1)} %param.19), kind=kLoop, calls=%fused_computation.54 | loop fusion | flops 810942 | bytes 270600 | tf_op jit(solution)/shard_map/reduce_sum | solution.py:22
  3.4 1.4 %convolution_convert_fusion.2 = bf16[66,64]{1,0:T(8,128)(2,1)S(1)} fusion(bf16[2048,64]{0,1:T(8,128)(2,1)} %param.24, f32[2048]{0:T(1024)} %param.21, f32[66]{0:T(128)S(1)} %add_rsqrt_fusion, bf16[2,2048]{1,0:T(2,128)(2,1)} %param.20, bf16[64,2048]{1,0:T(8,128)(2,1)} %param.19), kind=kOutput, calls=%fused_computation.45 | convolution fusion | flops 18251904 | bytes 549384 | tf_op jit(solution)/shard_map/dot_general | solution.py:123
  4.8 1.4 %convolution_convert_fusion.3 = bf16[66,64]{1,0:T(8,128)(2,1)S(1)} fusion(bf16[2048,64]{0,1:T(8,128)(2,1)} %param.23, f32[2048]{0:T(1024)} %param.21, f32[66]{0:T(128)S(1)} %add_rsqrt_fusion, bf16[2,2048]{1,0:T(2,128)(2,1)} %param.20, bf16[64,2048]{1,0:T(8,128)(2,1)} %param.19), kind=kOutput, calls=%fused_computation.46 | convolution fusion | flops 18251904 | bytes 549384 | tf_op jit(solution)/shard_map/dot_general | solution.py:122
  6.3 0.4 convolution_convert_fusion.1
  7.6 12.6 %all-gather = f32[4,1,4]{2,1,0:T(1,128)S(1)} all-gather(f32[1,1,4]{2,1,0:T(1,128)S(1)} %slice_bitcast_fusion.7), channel_id=1, replica_groups=mesh['grp'=2,'kv'=4,'tp'=4] {'kv'}, dimensions={0}, use_global_device_ids=true | all-gather | bytes 80 | tf_op jit(solution)/shard_map/all_gather | solution.py:9
  20.9 13.2 %all-gather.1 = f32[4,832,4]{1,2,0:T(4,128)S(1)} all-gather(f32[1,832,4]{1,2,0:T(4,128)S(1)} %maximum_bitcast_fusion), channel_id=1, replica_groups=mesh['grp'=2,'kv'=4,'tp'=4] {'kv'}, dimensions={0}, use_global_device_ids=true | all-gather | bytes 66560 | tf_op jit(solution)/shard_map/all_gather | solution.py:141
  34.2 0.6 fusion.55
  35.6 0.6 fusion.31
  36.4 17.8 %all_gather.9 = bf16[3328,1,128]{2,0,1:T(8,128)(2,1)S(1)} all-gather(bf16[832,1,128]{2,0,1:T(8,128)(2,1)S(1)} %maximum_maximum_fusion), channel_id=1, replica_groups=mesh['grp'=2,'kv'=4,'tp'=4] {'kv'}, dimensions={0}, use_global_device_ids=true | all-gather | bytes 1064960 | tf_op jit(solution)/shard_map/all_gather | solution.py:150
  54.2 14.4 %while.32 = (s32[]{:T(128)}, f32[64,1,4]{0,2,1:T(4,128)S(1)}, f32[64,1,4]{0,2,1:T(4,128)S(1)}, f32[64,1,4,64]{0,3,2,1:T(8,128)S(1)}, s32[4]{0:T(128)S(1)}, /*ind...) while((s32[]{:T(128)}, f32[64,1,4]{0,2,1:T(4,128)S(1)}, ...), condition=%wide.region_7.8_spmd.clone, body=%wide.region_4.7_spmd.clone.sunk | while | flops 56406536 | bytes 4148079 | solution.py:168
  54.2 0.6 dynamic_slice.48
  56.6 0.4 fusion.70
  56.9 0.3 fusion.72
  57.3 0.5 fusion.74
  57.9 0.6 dynamic_slice.48
  60.2 0.4 fusion.70
  60.6 0.3 fusion.72
  60.9 0.5 fusion.74
  61.5 0.6 dynamic_slice.48
  63.8 0.4 fusion.70
  64.5 0.5 fusion.74
  65.1 0.6 dynamic_slice.48
  67.4 0.4 fusion.70
  68.1 0.5 fusion.74
  68.9 3.7 %collective-permute-done = bf16[66,256]{0,1:T(8,128)(2,1)S(1)} collective-permute-done((bf16[66,256]{0,1:T(8,128)(2,1)S(1)}, bf16[66,256]{0,1:T(8,128)(2,1)S(1)}, u32[]{:S(2)}, u32[]{:S(2)}) %collective-permute-start) | collective-permute-done | bytes 33824 | tf_op jit(solution)/shard_map/ppermute | solution.py:189
  72.6 3.7 %collective-permute-done.1 = bf16[66,256]{0,1:T(8,128)(2,1)S(1)} collective-permute-done((bf16[66,256]{0,1:T(8,128)(2,1)S(1)}, bf16[66,256]{0,1:T(8,128)(2,1)S(1)}, u32[]{:S(2)}, u32[]{:S(2)}) %collective-permute-start.1) | collective-permute-done | bytes 33824 | tf_op jit(solution)/shard_map/ppermute | solution.py:189
  76.2 3.7 %collective-permute-done.2 = bf16[66,256]{0,1:T(8,128)(2,1)S(1)} collective-permute-done((bf16[66,256]{0,1:T(8,128)(2,1)S(1)}, bf16[66,256]{0,1:T(8,128)(2,1)S(1)}, u32[]{:S(2)}, u32[]{:S(2)}) %collective-permute-start.2) | collective-permute-done | bytes 33824 | tf_op jit(solution)/shard_map/ppermute | solution.py:189
  80.3 0.3 convolution_convert_fusion
  80.6 0.6 slice.76
  81.2 0.6 slice.75
  (123 shorter events, 5.5 us)
Async XLA Ops:
  0.6 79.6 %copy-start = (bf16[1024,512]{1,0:T(8,128)(2,1)S(1)}, bf16[1024,512]{1,0:T(8,128)(2,1)}, u32[]{:S(2)}) copy-start(bf16[1024,512]{1,0:T(8,128)(2,1)} %param.33) | copy-start | bytes 3145732
  0.6 5.6 %copy-start.6 = (bf16[2,2048]{1,0:T(2,128)(2,1)S(1)}, bf16[2,2048]{1,0:T(2,128)(2,1)}, u32[]{:S(2)}) copy-start(bf16[2,2048]{1,0:T(2,128)(2,1)} %param.20) | copy-start | bytes 24580
  0.7 5.6 %copy-start.3 = (bf16[64,2048]{1,0:T(8,128)(2,1)S(1)}, bf16[64,2048]{1,0:T(8,128)(2,1)}, u32[]{:S(2)}) copy-start(bf16[64,2048]{1,0:T(8,128)(2,1)} %param.19) | copy-start | bytes 786436
  0.7 5.6 %copy-start.10 = (f32[2048]{0:T(1024)S(1)}, f32[2048]{0:T(1024)}, u32[]{:S(2)}) copy-start(f32[2048]{0:T(1024)} %param.21) | copy-start | bytes 24580
  0.7 5.6 %copy-start.8 = (bf16[2048,256]{1,0:T(8,128)(2,1)S(1)}, bf16[2048,256]{1,0:T(8,128)(2,1)}, u32[]{:S(2)}) copy-start(bf16[2048,256]{1,0:T(8,128)(2,1)} %param.22) | copy-start | bytes 3145732
  4.8 2.0 %copy-start.9 = (bf16[2048,4]{0,1:T(4,128)(2,1)S(1)}, bf16[2048,4]{0,1:T(4,128)(2,1)}, u32[]{:S(2)}) copy-start(bf16[2048,4]{0,1:T(4,128)(2,1)} %param.25) | copy-start | bytes 49156
  4.8 2.0 %copy-start.11 = (f32[4]{0:T(128)S(1)}, f32[4]{0:T(128)}, u32[]{:S(2)}) copy-start(f32[4]{0:T(128)} %param.26) | copy-start | bytes 52
  4.8 2.3 %copy-start.7 = (f32[4,64]{1,0:T(4,128)S(1)}, f32[4,64]{1,0:T(4,128)}, u32[]{:S(2)}) copy-start(f32[4,64]{1,0:T(4,128)} %param.27) | copy-start | bytes 3076
  6.2 1.1 %copy-start.2 = (f32[2,4,3072]{2,1,0:T(4,128)S(1)}, f32[2,4,3072]{2,1,0:T(4,128)}, u32[]{:S(2)}) copy-start(f32[2,4,3072]{2,1,0:T(4,128)} %param.31) | copy-start | bytes 294916
  6.3 14.6 %copy-start.5 = (f32[4,768]{1,0:T(4,128)S(1)}, f32[4,768]{1,0:T(4,128)}, u32[]{:S(2)}) copy-start(f32[4,768]{1,0:T(4,128)} %param.29) | copy-start | bytes 36868
  6.3 27.9 %copy-start.1 = (bf16[2,3072,1,128]{3,1,2,0:T(8,128)(2,1)S(1)}, bf16[2,3072,1,128]{3,1,2,0:T(8,128)(2,1)}, u32[]{:S(2)}) copy-start(bf16[2,3072,1,128]{3,1,2,0:T(8,128)(2,1)} %param.30) | copy-start | bytes 4718596
  34.2 2.2 %copy-start.4 = (bf16[768,1,128]{2,0,1:T(8,128)(2,1)S(1)}, bf16[768,1,128]{2,0,1:T(8,128)(2,1)}, u32[]{:S(2)}) copy-start(bf16[768,1,128]{2,0,1:T(8,128)(2,1)} %param.28) | copy-start | bytes 589828
  68.8 3.7 %collective-permute-start = (bf16[66,256]{0,1:T(8,128)(2,1)S(1)}, bf16[66,256]{0,1:T(8,128)(2,1)S(1)}, u32[]{:S(2)}, u32[]{:S(2)}) collective-permute-start(bf16[66,256]{0,1:T(8,128)(2,1)S(1)} %pad_maximum_fusion.1), channel_id=1, source_target_pairs={{0,1},{1,2},{2,3},{3,0},{4,5},{5,6},{6,7},{7,4},{8,9},{9,10},{10,1... | collective-permute-start | bytes 101384 | tf_op jit(solution)/shard_map/ppermute | solution.py:189
  72.5 3.7 %collective-permute-start.1 = (bf16[66,256]{0,1:T(8,128)(2,1)S(1)}, bf16[66,256]{0,1:T(8,128)(2,1)S(1)}, u32[]{:S(2)}, u32[]{:S(2)}) collective-permute-start(bf16[66,256]{0,1:T(8,128)(2,1)S(1)} %collective-permute-done), channel_id=1, source_target_pairs={{0,1},{1,2},{2,3},{3,0},{4,5},{5,6},{6,7},{7,4},{8,9},{9,10},{10,1... | collective-permute-start | bytes 101384 | tf_op jit(solution)/shard_map/ppermute | solution.py:189
  76.2 3.7 %collective-permute-start.2 = (bf16[66,256]{0,1:T(8,128)(2,1)S(1)}, bf16[66,256]{0,1:T(8,128)(2,1)S(1)}, u32[]{:S(2)}, u32[]{:S(2)}) collective-permute-start(bf16[66,256]{0,1:T(8,128)(2,1)S(1)} %collective-permute-done.1), channel_id=1, source_target_pairs={{0,1},{1,2},{2,3},{3,0},{4,5},{5,6},{6,7},{7,4},{8,9},{9,10},{10,1... | collective-permute-start | bytes 101384 | tf_op jit(solution)/shard_map/ppermute | solution.py:189
